TPU v7x, 32 devices: a whole 2x2x4 slice. The times are simulated.
32 devices in a mesh: ep: 16 (over z, x, core), tp: 2 (over y).
Axes of the slice: x: 2, y: 2, z: 4, core: 2. Of those that a mesh axis runs over, the one named last changes fastest.
Arguments:
- tokens: bfloat16 [2048, 2048], P('ep'), may hold values from -6 to 6
- cotangent: bfloat16 [2048, 2048], P('ep'), may hold values from -1.796875 to 1.796875
- group_weight: float32 [2048], P('ep'), may hold values from 0.2 to 1
- expert_weight: float32 [2048, 2], P('ep'), may hold values from 0.1 to 0.9
- group_choice: int32 [2048], P('ep'), may hold values from 0 to 3, as said below
- local_choice: int32 [2048, 2], P('ep'), may hold values from 0 to 3, as said below
- w_gate: bfloat16 [16, 2048, 512], P('ep', None, 'tp'), may hold values from -0.125 to 0.125
- w_up: bfloat16 [16, 2048, 512], P('ep', None, 'tp'), may hold values from -0.125 to 0.125
- w_down: bfloat16 [16, 512, 2048], P('ep', 'tp'), may hold values from -0.25 to 0.25
Outputs:
- token_grad: float32 [2048, 2048], P('ep', 'tp')
- group_weight_grad: float32 [2048], P('ep')
- expert_weight_grad: float32 [2048, 2], P('ep')
- w_gate_grad: float32 [16, 2048, 512], P('ep', None, 'tp')
- w_up_grad: float32 [16, 2048, 512], P('ep', None, 'tp')
- w_down_grad: float32 [16, 512, 2048], P('ep', 'tp')
Inputs may be any that keep to these rules, and one draw needn't show every extreme that they name: Among the 128 tokens of each device (aligned blocks of tokens), no expert 4 * group_choice + local_choice is named by more than 24 slots, and some expert is named by exactly 24 slots of every device. `local_choice`: the 2 local choices of a token differ.
All inputs are finite; a program needn't handle non-finite values.
Results may differ from a plain program's by a relative error of at most 0.006.
Values may be sent and summed in bfloat16 or wider, within the bound.
A program may use at most 64 MiB of HBM per device.

v0:
```python
import jax
import jax.numpy as jnp
from jax import lax
from jax.sharding import PartitionSpec as P

EPG = 4


def shards(
    tokens, cotangent, group_weight, expert_weight, group_choice, local_choice, w_gate, w_up, w_down
):
    token_count, feature_count = tokens.shape
    pick_count = expert_weight.shape[1]
    expert_count = lax.axis_size("ep")
    lane_count = lax.axis_size("tp")
    slot_count = token_count * pick_count
    capacity = pick_count * (3 * token_count // (2 * expert_count))
    buffer_count = expert_count * capacity
    piece_width = feature_count // lane_count
    expert_of = (group_choice[:, None] * EPG + local_choice).reshape(slot_count)
    member = (expert_of[:, None] == jnp.arange(expert_count, dtype=jnp.int32)[None, :]).astype(
        jnp.bfloat16
    )
    order = jnp.arange(slot_count, dtype=jnp.int32)
    earlier_mask = (order[:, None] > order[None, :]).astype(jnp.bfloat16)
    earlier = jnp.dot(earlier_mask, member, preferred_element_type=jnp.float32)
    position = jnp.sum(earlier * member.astype(jnp.float32), axis=1).astype(jnp.int32)
    slot_index = expert_of * capacity + position
    owner = (
        jnp.full((buffer_count,), token_count, jnp.int32).at[slot_index].set(order // pick_count)
    )
    gate_value = (group_weight[:, None] * expert_weight).astype(jnp.bfloat16).reshape(slot_count)
    gate_buffer = jnp.zeros((buffer_count,), jnp.bfloat16).at[slot_index].set(gate_value)
    start = lax.axis_index("tp") * piece_width
    token_cols = lax.dynamic_slice_in_dim(tokens, start, piece_width, 1)
    cot_cols = lax.dynamic_slice_in_dim(cotangent, start, piece_width, 1)
    token_part = jnp.take(token_cols, owner, axis=0, mode="fill", fill_value=0)
    cot_part = jnp.take(cot_cols, owner, axis=0, mode="fill", fill_value=0)
    token_part, gate_rows, cot_part = (
        lax.all_to_all(token_part, "ep", split_axis=0, concat_axis=0, tiled=True),
        lax.all_to_all(gate_buffer, "ep", split_axis=0, concat_axis=0, tiled=True),
        lax.all_to_all(cot_part, "ep", split_axis=0, concat_axis=0, tiled=True),
    )
    arrived, cot_rows = (
        lax.all_gather(token_part, "tp", axis=1, tiled=True),
        lax.all_gather(cot_part, "tp", axis=1, tiled=True),
    )
    first = w_gate[0]
    second = w_up[0]
    third = w_down[0]
    contract_cols = (((1,), (1,)), ((), ()))
    contract_rows = (((0,), (0,)), ((), ()))
    pre_gate = jnp.dot(arrived, first, preferred_element_type=jnp.float32)
    pre_up = jnp.dot(arrived, second, preferred_element_type=jnp.float32)
    back_hidden = lax.dot_general(
        cot_rows, third, contract_cols, preferred_element_type=jnp.float32
    )
    sigma = jax.nn.sigmoid(pre_gate)
    swish = pre_gate * sigma
    hidden = swish * pre_up
    gate_part = jnp.sum(hidden * back_hidden, axis=1)
    gate_float = gate_rows.reshape(buffer_count, 1).astype(jnp.float32)
    scaled = gate_float * back_hidden
    grad_gate_pre = (scaled * pre_up * sigma * (1.0 + pre_gate * (1.0 - sigma))).astype(
        jnp.bfloat16
    )
    grad_up_pre = (scaled * swish).astype(jnp.bfloat16)
    weighted = (gate_float * hidden).astype(jnp.bfloat16)
    first_grad = lax.dot_general(
        arrived, grad_gate_pre, contract_rows, preferred_element_type=jnp.float32
    )
    second_grad = lax.dot_general(
        arrived, grad_up_pre, contract_rows, preferred_element_type=jnp.float32
    )
    third_grad = lax.dot_general(
        weighted, cot_rows, contract_rows, preferred_element_type=jnp.float32
    )
    partial_value = lax.dot_general(
        grad_gate_pre, first, contract_cols, preferred_element_type=jnp.float32
    )
    partial_value = partial_value + lax.dot_general(
        grad_up_pre, second, contract_cols, preferred_element_type=jnp.float32
    )
    pieces = lax.all_to_all(partial_value, "tp", split_axis=1, concat_axis=0, tiled=True)
    row_grad = jnp.sum(pieces.reshape(lane_count, buffer_count, piece_width), axis=0).astype(
        jnp.bfloat16
    )
    gate_total = lax.psum(gate_part, "tp").astype(jnp.bfloat16)
    returned, gate_back = (
        lax.all_to_all(row_grad, "ep", split_axis=0, concat_axis=0, tiled=True),
        lax.all_to_all(gate_total, "ep", split_axis=0, concat_axis=0, tiled=True),
    )
    slot_grad = jnp.take(returned, slot_index, axis=0).astype(jnp.float32)
    token_grad = jnp.sum(slot_grad.reshape(token_count, pick_count, piece_width), axis=1)
    gate_grad = (
        jnp.take(gate_back, slot_index, axis=0).astype(jnp.float32).reshape(token_count, pick_count)
    )
    group_grad = jnp.sum(expert_weight * gate_grad, axis=1)
    expert_grad = group_weight[:, None] * gate_grad
    return (
        token_grad,
        group_grad,
        expert_grad,
        first_grad[None],
        second_grad[None],
        third_grad[None],
    )


def solution(mesh):
    in_specs = (
        P("ep", None),
        P("ep", None),
        P("ep"),
        P("ep", None),
        P("ep"),
        P("ep", None),
        P("ep", None, "tp"),
        P("ep", None, "tp"),
        P("ep", "tp", None),
    )
    out_specs = (
        P("ep", "tp"),
        P("ep"),
        P("ep", None),
        P("ep", None, "tp"),
        P("ep", None, "tp"),
        P("ep", "tp", None),
    )
    return jax.shard_map(shards, mesh=mesh, in_specs=in_specs, out_specs=out_specs, check_vma=False)
```

profile of v0, /device:TPU:9, one launch (start us, length us, event | category | flops | bytes accessed | tf_op | source)
XLA Modules:
  0.0 192.6 jit_solution(5820197067806515921)
XLA Ops:
  9.4 1.4 scatter_custom_fusion.1
  11.9 2.1 %gather_fusion.3 = bf16[384,1024]{1,0:T(8,128)(2,1)S(1)} fusion(bf16[128,1024]{1,0:T(8,128)(2,1)S(1)} %get-tuple-element.28, s32[1024]{0:T(1024)S(1)} %pad_clamp_fusion.1), kind=kCustom, calls=%fused_computation.1.clone | custom fusion | bytes 1574400 | tf_op jit(solution)/shard_map/jit(_take)/gather | solution.py:37
  14.0 2.1 %gather_fusion.2 = bf16[384,1024]{1,0:T(8,128)(2,1)S(1)} fusion(bf16[128,1024]{1,0:T(8,128)(2,1)S(1)} %get-tuple-element.29, s32[1024]{0:T(1024)S(1)} %pad_clamp_fusion.1), kind=kCustom, calls=%fused_computation.clone | custom fusion | bytes 1574400 | tf_op jit(solution)/shard_map/jit(_take)/gather | solution.py:38
  16.2 26.4 %all_to_all.69 = bf16[16,24,1024]{2,1,0:T(8,128)(2,1)} all-to-all(bf16[16,24,1024]{2,1,0:T(8,128)(2,1)S(1)} %bitcast.50), channel_id=1, replica_groups=mesh['ep'=16,'tp'=2] {'ep'}, dimensions={0} | all-to-all | bytes 1572864 | tf_op jit(solution)/shard_map/all_to_all | solution.py:40
  42.7 24.0 %all_to_all.70 = bf16[16,24,1024]{2,1,0:T(8,128)(2,1)} all-to-all(bf16[16,24,1024]{2,1,0:T(8,128)(2,1)S(1)} %bitcast.49), channel_id=1, replica_groups=mesh['ep'=16,'tp'=2] {'ep'}, dimensions={0} | all-to-all | bytes 1572864 | tf_op jit(solution)/shard_map/all_to_all | solution.py:42
  67.0 2.2 %scatter_custom_fusion = bf16[384]{0:T(512)(128)(2,1)S(1)} fusion(s32[256]{0:T(256)S(1)} %bitcast.53, bf16[256]{0:T(256)(128)(2,1)S(1)} %reshape.142, bf16[]{:T(256)} %constant.47.clone.1), kind=kCustom, calls=%fused_computation.58 | custom fusion | bytes 770 | tf_op jit(solution)/shard_map/scatter | solution.py:33
  69.3 8.7 %all_to_all.71 = bf16[16,24,1]{1,2,0:T(2,128)(2,1)S(1)} all-to-all(bf16[16,24,1]{1,2,0:T(2,128)(2,1)S(1)} %all_to_all.61), channel_id=1, replica_groups=mesh['ep'=16,'tp'=2] {'ep'}, dimensions={0} | all-to-all | bytes 1536 | tf_op jit(solution)/shard_map/all_to_all | solution.py:41
  78.1 2.3 %fusion.3 = f32[384,256]{0,1:T(8,128)S(1)} fusion(bf16[384,2048]{1,0:T(8,128)(2,1)} %all-gather.5.cloned.1.call-done, bf16[1,2048,256]{2,1,0:T(8,128)(2,1)S(1)} %copy-done), kind=kOutput, calls=%fused_computation.15 | convolution fusion | flops 402653184 | bytes 3014656 | tf_op jit(solution)/shard_map/dot_general | solution.py:53
  80.5 2.1 %fusion.6 = f32[384,256]{0,1:T(8,128)S(1)} fusion(bf16[384,2048]{1,0:T(8,128)(2,1)S(1)} %copy-done.1, bf16[1,2048,256]{2,1,0:T(8,128)(2,1)} %param.18), kind=kOutput, calls=%fused_computation.18 | convolution fusion | flops 402653184 | bytes 3014656 | tf_op jit(solution)/shard_map/dot_general | solution.py:54
  82.6 14.8 %all-gather.3.cloned.1.call-done = bf16[384,2048]{1,0:T(8,128)(2,1)} async-done(((bf16[384,1024]{1,0:T(8,128)(2,1)}), bf16[384,2048]{1,0:T(8,128)(2,1)}) %all-gather.3.cloned.1.call-update) | async-done | bytes 1572880 | tf_op jit(solution)/shard_map/all_gather | solution.py:46
  97.4 2.5 %multiply_reduce_fusion = (f32[384]{0:T(512)S(1)}, bf16[384,256]{0,1:T(8,128)(2,1)S(1)}, bf16[384,256]{0,1:T(8,128)(2,1)S(1)}) fusion(f32[384,256]{0,1:T(8,128)S(1)} %fusion.6, f32[384,256]{0,1:T(8,128)S(1)} %fusion.3, f32[384]{0:T(512)S(1)} %reshape.105, bf16[384,2048]{1,0:T(8,128)(2,1)} %all-gather.3.cloned.1.call-done, bf16[1,256,2048]{2,1,0:T(8,128)(2,1)} %param.19), kind=kOutput, calls=%fused_computation.27 | convolution fusion | flops 404323968 | bytes 3804160 | tf_op jit(solution)/shard_map/dot_general | solution.py:55
  101.9 1.9 copy.31
  103.8 5.2 %all-to-all-start.3 = ((f32[384,2,1024]{2,0,1:T(8,128)}), f32[384,2,1024]{2,0,1:T(8,128)}, u32[]{:S(2)}, u32[]{:S(2)}) async-start(f32[384,2,1024]{2,0,1:T(8,128)} %bitcast.45), calls=%async_computation.3 | async-start | bytes 6291456 | tf_op jit(solution)/shard_map/all_to_all | solution.py:84
  109.0 35.5 %psum.7 = bf16[384]{0:T(512)(128)(2,1)S(1)} all-reduce(f32[384]{0:T(512)S(1)} %get-tuple-element.23), channel_id=1, replica_groups=mesh['ep'=16,'tp'=2] {'tp'}, use_global_device_ids=true, to_apply=%region_6.8 | all-reduce | flops 384 | bytes 2304 | tf_op jit(solution)/shard_map/psum | solution.py:88
  145.3 7.3 %all-to-all-start.5 = ((bf16[16,24,1]{1,2,0:T(2,128)(2,1)}), bf16[16,24,1]{1,2,0:T(2,128)(2,1)S(1)}, u32[]{:S(2)}, u32[]{:S(2)}) async-start(bf16[16,24,1]{1,2,0:T(2,128)(2,1)} %all_to_all.62), calls=%async_computation.5 | async-start | bytes 16384 | tf_op jit(solution)/shard_map/all_to_all | solution.py:91
  152.6 3.3 %reduce_sum.46 = bf16[384,1024]{1,0:T(8,128)(2,1)} reduce(f32[384,2,1024]{2,0,1:T(8,128)} %all-to-all-done.3, f32[]{:T(128)} %constant.43.clone.1), dimensions={1}, to_apply=%region_3.5 | reduce | flops 393216 | bytes 3932164 | tf_op jit(solution)/shard_map/reduce_sum | solution.py:85
  155.8 1.4 all-to-all-done.5
  157.3 5.2 %all-to-all-start.4 = ((bf16[16,24,1024]{2,1,0:T(8,128)(2,1)}), bf16[16,24,1024]{2,1,0:T(8,128)(2,1)S(1)}, u32[]{:S(2)}, u32[]{:S(2)}) async-start(bf16[16,24,1024]{2,1,0:T(8,128)(2,1)} %bitcast.48), calls=%async_computation.4 | async-start | bytes 1572864 | tf_op jit(solution)/shard_map/all_to_all | solution.py:90
  164.0 3.0 %convolution_bitcast_fusion.1 = f32[1,2048,256]{2,1,0:T(8,128)} fusion(bf16[384,2048]{1,0:T(8,128)(2,1)S(1)} %copy-done.1, bf16[384,256]{0,1:T(8,128)(2,1)} %copy-done.10), kind=kOutput, calls=%fused_computation.9 | convolution fusion | flops 402653184 | bytes 3866624 | tf_op jit(solution)/shard_map/dot_general | solution.py:72
  167.1 2.1 %convolution_bitcast_fusion.2 = f32[1,2048,256]{2,1,0:T(8,128)} fusion(bf16[384,2048]{1,0:T(8,128)(2,1)S(1)} %copy-done.1, bf16[384,256]{0,1:T(8,128)(2,1)S(1)} %copy-done.9), kind=kOutput, calls=%fused_computation.10 | convolution fusion | flops 402653184 | bytes 3866624 | tf_op jit(solution)/shard_map/dot_general | solution.py:69
  169.2 2.1 %convolution_bitcast_fusion = f32[1,256,2048]{2,1,0:T(8,128)} fusion(bf16[384,2048]{1,0:T(8,128)(2,1)S(1)} %copy-done.3, f32[384]{0:T(512)S(1)} %reshape.105, f32[384,256]{0,1:T(8,128)S(1)} %copy-done.7, f32[384,256]{0,1:T(8,128)S(1)} %copy-done.5), kind=kOutput, calls=%fused_computation.8 | convolution fusion | flops 403341312 | bytes 4457984 | tf_op jit(solution)/shard_map/dot_general | solution.py:75
  171.4 1.9 %gather_fusion.1 = bf16[256]{0:T(256)(128)(2,1)S(1)} fusion(bf16[384]{0:T(512)(128)(2,1)S(1)} %all_to_all.60, s32[1024]{0:T(1024)S(1)} %pad_clamp_fusion), kind=kCustom, calls=%fused_computation.3 | custom fusion | bytes 2048 | tf_op jit(solution)/shard_map/jit(_take)/gather | solution.py:96
  174.9 7.3 %all-to-all-done.4 = bf16[16,24,1024]{2,1,0:T(8,128)(2,1)S(1)} async-done(((bf16[16,24,1024]{2,1,0:T(8,128)(2,1)}), bf16[16,24,1024]{2,1,0:T(8,128)(2,1)S(1)}, u32[]{:S(2)}, u32[]{:S(2)}) %all-to-all-start.4) | async-done | bytes 786464 | tf_op jit(solution)/shard_map/all_to_all | solution.py:90
  183.5 2.2 %convert_reduce_fusion = f32[128,1024]{1,0:T(8,128)} fusion(bf16[128,2,1024]{2,1,0:T(2,128)(2,1)S(1)} %gather.16, pred[128,2]{1,0:T(8,128)(4,1)S(1)} %get-tuple-element.20), kind=kLoop, calls=%fused_computation.22 | loop fusion | flops 655360 | bytes 1048832 | tf_op jit(solution)/shard_map/reduce_sum | solution.py:94
  (72 shorter events, 11.3 us)
Async XLA Ops:
  7.2 70.9 %copy-start = (bf16[1,2048,256]{2,1,0:T(8,128)(2,1)S(1)}, bf16[1,2048,256]{2,1,0:T(8,128)(2,1)}, u32[]{:S(2)}) copy-start(bf16[1,2048,256]{2,1,0:T(8,128)(2,1)} %param.17) | copy-start | bytes 3145732
  7.2 70.9 %all-gather.5.cloned.1.call-start = ((), (), s32[]{:S(2)}) async-start(), calls=%async_computation.7 | async-start | bytes 2359296 | tf_op jit(solution)/shard_map/all_gather | solution.py:45
  9.4 57.6 %copy-start.13 = (s32[256,1]{0,1:T(1,128)}, s32[256,1]{0,1:T(1,128)S(1)}, u32[]{:S(2)}) copy-start(s32[256,1]{0,1:T(1,128)S(1)} %compare_select_fusion.1) | copy-start | bytes 3076
  42.6 24.1 %copy-start.12 = (f32[128,2]{0,1:T(2,128)S(1)}, f32[128,2]{0,1:T(2,128)}, u32[]{:S(2)}) copy-start(f32[128,2]{0,1:T(2,128)} %param.14) | copy-start | bytes 3076
  42.6 24.1 %copy-start.14 = (f32[128]{0:T(128)S(1)}, f32[128]{0:T(128)}, u32[]{:S(2)}) copy-start(f32[128]{0:T(128)} %param.13) | copy-start | bytes 1540
  42.6 54.7 %all-gather.3.cloned.1.call-start = ((), (), s32[]{:S(2)}) async-start(), calls=%async_computation.6 | async-start | bytes 2359296 | tf_op jit(solution)/shard_map/all_gather | solution.py:46
  78.1 2.3 %copy-start.1 = (bf16[384,2048]{1,0:T(8,128)(2,1)S(1)}, bf16[384,2048]{1,0:T(8,128)(2,1)}, u32[]{:S(2)}) copy-start(bf16[384,2048]{1,0:T(8,128)(2,1)} %all-gather.5.cloned.1.call-done) | copy-start | bytes 4718596
  80.5 19.4 %copy-start.4 = (f32[384,256]{0,1:T(8,128)}, f32[384,256]{0,1:T(8,128)S(1)}, u32[]{:S(2)}) copy-start(f32[384,256]{0,1:T(8,128)S(1)} %fusion.3) | copy-start | bytes 1179652
  82.6 17.3 %copy-start.6 = (f32[384,256]{0,1:T(8,128)}, f32[384,256]{0,1:T(8,128)S(1)}, u32[]{:S(2)}) copy-start(f32[384,256]{0,1:T(8,128)S(1)} %fusion.6) | copy-start | bytes 1179652
  99.9 0.7 copy-start.8
  99.9 0.7 copy-start.10
  99.9 1.4 copy-start.2
  103.8 41.4 %all-to-all-start.3 = ((f32[384,2,1024]{2,0,1:T(8,128)}), f32[384,2,1024]{2,0,1:T(8,128)}, u32[]{:S(2)}, u32[]{:S(2)}) async-start(f32[384,2,1024]{2,0,1:T(8,128)} %bitcast.45), calls=%async_computation.3 | async-start | bytes 6291456 | tf_op jit(solution)/shard_map/all_to_all | solution.py:84
  145.3 12.0 %all-to-all-start.5 = ((bf16[16,24,1]{1,2,0:T(2,128)(2,1)}), bf16[16,24,1]{1,2,0:T(2,128)(2,1)S(1)}, u32[]{:S(2)}, u32[]{:S(2)}) async-start(bf16[16,24,1]{1,2,0:T(2,128)(2,1)} %all_to_all.62), calls=%async_computation.5 | async-start | bytes 16384 | tf_op jit(solution)/shard_map/all_to_all | solution.py:91
  157.3 24.9 %all-to-all-start.4 = ((bf16[16,24,1024]{2,1,0:T(8,128)(2,1)}), bf16[16,24,1024]{2,1,0:T(8,128)(2,1)S(1)}, u32[]{:S(2)}, u32[]{:S(2)}) async-start(bf16[16,24,1024]{2,1,0:T(8,128)(2,1)} %bitcast.48), calls=%async_computation.4 | async-start | bytes 1572864 | tf_op jit(solution)/shard_map/all_to_all | solution.py:90
  164.0 3.0 %copy-start.9 = (bf16[384,256]{0,1:T(8,128)(2,1)S(1)}, bf16[384,256]{0,1:T(8,128)(2,1)}, u32[]{:S(2)}) copy-start(bf16[384,256]{0,1:T(8,128)(2,1)} %copy-done.8) | copy-start | bytes 589828
  167.1 2.1 %copy-start.3 = (bf16[384,2048]{1,0:T(8,128)(2,1)S(1)}, bf16[384,2048]{1,0:T(8,128)(2,1)}, u32[]{:S(2)}) copy-start(bf16[384,2048]{1,0:T(8,128)(2,1)} %all-gather.3.cloned.1.call-done) | copy-start | bytes 4718596
  167.1 2.1 %copy-start.5 = (f32[384,256]{0,1:T(8,128)S(1)}, f32[384,256]{0,1:T(8,128)}, u32[]{:S(2)}) copy-start(f32[384,256]{0,1:T(8,128)} %copy-done.4) | copy-start | bytes 1179652
  167.1 2.1 %copy-start.7 = (f32[384,256]{0,1:T(8,128)S(1)}, f32[384,256]{0,1:T(8,128)}, u32[]{:S(2)}) copy-start(f32[384,256]{0,1:T(8,128)} %copy-done.6) | copy-start | bytes 1179652
  169.2 4.3 %copy-start.11 = (s32[128,2]{1,0:T(8,128)S(1)}, s32[128,2]{1,0:T(8,128)}, u32[]{:S(2)}) copy-start(s32[128,2]{1,0:T(8,128)} %convert_element_type.71) | copy-start | bytes 3076
  169.2 4.3 %copy-start.15 = (f32[128]{0:T(128)S(1)}, f32[128]{0:T(128)}, u32[]{:S(2)}) copy-start(f32[128]{0:T(128)} %param.13) | copy-start | bytes 1540
Sparse Core Ops, SparseCore 0:
  42.7 25.8 all-gather.4
  70.2 27.1 all-gather.2
where the time goes:
time: 193 us
  blocking collectives  94.5 us (49%)
  waiting for transfers between devices  23.5 us (12%)
  local copies, waits for them, and re-layouts  18.8 us (10%)
  starting transfers between devices  17.8 us (9%)
  matrix products  15.6 us (8%)
  between operations  14.4 us (7%)
  other arithmetic  7.91 us (4%)
    psum x1, blocking collectives, shards(): gate_total = lax.psum(gate_part, 'tp').astype(jnp.bfloat16)  35.5 us
    all_to_all x1, blocking collectives, shards(): lax.all_to_all(token_part, 'ep', split_axis=0, concat_axis=0, tiled=True)  26.4 us
    all_to_all x1, blocking collectives, shards(): lax.all_to_all(cot_part, 'ep', split_axis=0, concat_axis=0, tiled=True)  24 us
    all_gather x1, waiting for transfers between devices, shards(): lax.all_gather(cot_part, 'tp', axis=1, tiled=True)  14.8 us
    all_to_all x1, blocking collectives, shards(): lax.all_to_all(gate_buffer, 'ep', split_axis=0, concat_axis=0, tiled=True)  8.69 us
    all_to_all x1, starting transfers between devices, shards(): lax.all_to_all(gate_total, 'ep', split_axis=0, concat_axis=0, tiled=True)  7.32 us
    all_to_all x1, waiting for transfers between devices, shards(): lax.all_to_all(row_grad, 'ep', split_axis=0, concat_axis=0, tiled=True)  7.25 us
    all_to_all x1, starting transfers between devices, shards(): lax.all_to_all(row_grad, 'ep', split_axis=0, concat_axis=0, tiled=True)  5.21 us
  transfers between devices with their start and end apart: 5, of which 3 were waited for; matrix products, arithmetic and copies ran while one was open for 12% of the time, Pallas kernels for 0%

commit v1 on v0

--- a/solution.py
+++ b/solution.py
@@ -85,7 +85,7 @@
     row_grad = jnp.sum(pieces.reshape(lane_count, buffer_count, piece_width), axis=0).astype(
         jnp.bfloat16
     )
-    gate_total = lax.psum(gate_part, "tp").astype(jnp.bfloat16)
+    gate_total = jnp.sum(lax.all_gather(gate_part, "tp"), axis=0).astype(jnp.bfloat16)
     returned, gate_back = (
         lax.all_to_all(row_grad, "ep", split_axis=0, concat_axis=0, tiled=True),
         lax.all_to_all(gate_total, "ep", split_axis=0, concat_axis=0, tiled=True),

time: 193 us -> 193 us (level)
    psum x1 -> x0, blocking collectives: 35.5 us -> none  [shards(): gate_total = lax.psum(gate_part, 'tp').astype(jnp.bfloat16)]
    all_gather x0 -> x1, blocking collectives: none -> 35.5 us  [shards(): lax.all_gather(gate_part, 'tp')]
where the time goes in v1:
time: 193 us
  blocking collectives  94.5 us (49%)
  waiting for transfers between devices  23.5 us (12%)
  local copies, waits for them, and re-layouts  18.8 us (10%)
  starting transfers between devices  17.8 us (9%)
  matrix products  15.6 us (8%)
  between operations  14.4 us (7%)
  other arithmetic  7.93 us (4%)
    all_gather x1, blocking collectives, shards(): lax.all_gather(gate_part, 'tp')  35.5 us
    all_to_all x1, blocking collectives, shards(): lax.all_to_all(token_part, 'ep', split_axis=0, concat_axis=0, tiled=True)  26.4 us
    all_to_all x1, blocking collectives, shards(): lax.all_to_all(cot_part, 'ep', split_axis=0, concat_axis=0, tiled=True)  24 us
    all_gather x1, waiting for transfers between devices, shards(): lax.all_gather(cot_part, 'tp', axis=1, tiled=True)  14.8 us
    all_to_all x1, blocking collectives, shards(): lax.all_to_all(gate_buffer, 'ep', split_axis=0, concat_axis=0, tiled=True)  8.69 us
    all_to_all x1, starting transfers between devices, shards(): lax.all_to_all(gate_total, 'ep', split_axis=0, concat_axis=0, tiled=True)  7.34 us
    all_to_all x1, waiting for transfers between devices, shards(): lax.all_to_all(row_grad, 'ep', split_axis=0, concat_axis=0, tiled=True)  7.25 us
    all_to_all x1, starting transfers between devices, shards(): lax.all_to_all(row_grad, 'ep', split_axis=0, concat_axis=0, tiled=True)  5.21 us
  transfers between devices with their start and end apart: 5, of which 3 were waited for; matrix products, arithmetic and copies ran while one was open for 12% of the time, Pallas kernels for 0%

profile of v1, /device:TPU:9, one launch (start us, length us, event | category | flops | bytes accessed | tf_op | source)
XLA Modules:
  0.0 192.6 jit_solution(14050100003820684092)
XLA Ops:
  9.4 1.4 scatter_custom_fusion.1
  11.9 2.1 %gather_fusion.3 = bf16[384,1024]{1,0:T(8,128)(2,1)S(1)} fusion(bf16[128,1024]{1,0:T(8,128)(2,1)S(1)} %get-tuple-element.28, s32[1024]{0:T(1024)S(1)} %pad_clamp_fusion.1), kind=kCustom, calls=%fused_computation.1.clone | custom fusion | bytes 1574400 | tf_op jit(solution)/shard_map/jit(_take)/gather | solution.py:37
  14.0 2.1 %gather_fusion.2 = bf16[384,1024]{1,0:T(8,128)(2,1)S(1)} fusion(bf16[128,1024]{1,0:T(8,128)(2,1)S(1)} %get-tuple-element.29, s32[1024]{0:T(1024)S(1)} %pad_clamp_fusion.1), kind=kCustom, calls=%fused_computation.clone | custom fusion | bytes 1574400 | tf_op jit(solution)/shard_map/jit(_take)/gather | solution.py:38
  16.2 26.4 %all_to_all.65 = bf16[16,24,1024]{2,1,0:T(8,128)(2,1)} all-to-all(bf16[16,24,1024]{2,1,0:T(8,128)(2,1)S(1)} %bitcast.50), channel_id=1, replica_groups=mesh['ep'=16,'tp'=2] {'ep'}, dimensions={0} | all-to-all | bytes 1572864 | tf_op jit(solution)/shard_map/all_to_all | solution.py:40
  42.7 24.0 %all_to_all.66 = bf16[16,24,1024]{2,1,0:T(8,128)(2,1)} all-to-all(bf16[16,24,1024]{2,1,0:T(8,128)(2,1)S(1)} %bitcast.49), channel_id=1, replica_groups=mesh['ep'=16,'tp'=2] {'ep'}, dimensions={0} | all-to-all | bytes 1572864 | tf_op jit(solution)/shard_map/all_to_all | solution.py:42
  67.0 2.2 %scatter_custom_fusion = bf16[384]{0:T(512)(128)(2,1)S(1)} fusion(s32[256]{0:T(256)S(1)} %bitcast.53, bf16[256]{0:T(256)(128)(2,1)S(1)} %reshape.153, bf16[]{:T(256)} %constant.47.clone.1), kind=kCustom, calls=%fused_computation.58 | custom fusion | bytes 770 | tf_op jit(solution)/shard_map/scatter | solution.py:33
  69.3 8.7 %all_to_all.67 = bf16[16,24,1]{1,2,0:T(2,128)(2,1)S(1)} all-to-all(bf16[16,24,1]{1,2,0:T(2,128)(2,1)S(1)} %all_to_all.58), channel_id=1, replica_groups=mesh['ep'=16,'tp'=2] {'ep'}, dimensions={0} | all-to-all | bytes 1536 | tf_op jit(solution)/shard_map/all_to_all | solution.py:41
  78.1 2.3 %fusion.3 = f32[384,256]{0,1:T(8,128)S(1)} fusion(bf16[384,2048]{1,0:T(8,128)(2,1)} %all-gather.7.cloned.1.call-done, bf16[1,2048,256]{2,1,0:T(8,128)(2,1)S(1)} %copy-done), kind=kOutput, calls=%fused_computation.15 | convolution fusion | flops 402653184 | bytes 3014656 | tf_op jit(solution)/shard_map/dot_general | solution.py:53
  80.5 2.1 %fusion.6 = f32[384,256]{0,1:T(8,128)S(1)} fusion(bf16[384,2048]{1,0:T(8,128)(2,1)S(1)} %copy-done.1, bf16[1,2048,256]{2,1,0:T(8,128)(2,1)} %param.18), kind=kOutput, calls=%fused_computation.18 | convolution fusion | flops 402653184 | bytes 3014656 | tf_op jit(solution)/shard_map/dot_general | solution.py:54
  82.6 14.8 %all-gather.5.cloned.1.call-done = bf16[384,2048]{1,0:T(8,128)(2,1)} async-done(((bf16[384,1024]{1,0:T(8,128)(2,1)}), bf16[384,2048]{1,0:T(8,128)(2,1)}) %all-gather.5.cloned.1.call-update) | async-done | bytes 1572880 | tf_op jit(solution)/shard_map/all_gather | solution.py:46
  97.4 2.5 %multiply_reduce_fusion = (f32[384]{0:T(512)S(1)}, bf16[384,256]{0,1:T(8,128)(2,1)S(1)}, bf16[384,256]{0,1:T(8,128)(2,1)S(1)}) fusion(f32[384,256]{0,1:T(8,128)S(1)} %fusion.6, f32[384,256]{0,1:T(8,128)S(1)} %fusion.3, f32[384]{0:T(512)S(1)} %reshape.116, bf16[384,2048]{1,0:T(8,128)(2,1)} %all-gather.5.cloned.1.call-done, bf16[1,256,2048]{2,1,0:T(8,128)(2,1)} %param.19), kind=kOutput, calls=%fused_computation.27 | convolution fusion | flops 404323968 | bytes 3804160 | tf_op jit(solution)/shard_map/dot_general | solution.py:55
  101.9 1.9 copy.31
  103.8 5.2 %all-to-all-start.3 = ((f32[384,2,1024]{2,0,1:T(8,128)}), f32[384,2,1024]{2,0,1:T(8,128)}, u32[]{:S(2)}, u32[]{:S(2)}) async-start(f32[384,2,1024]{2,0,1:T(8,128)} %bitcast.45), calls=%async_computation.3 | async-start | bytes 6291456 | tf_op jit(solution)/shard_map/all_to_all | solution.py:84
  109.0 35.5 %all-gather.1 = f32[2,1,384]{2,1,0:T(1,128)S(1)} all-gather(f32[1,1,384]{2,1,0:T(1,128)S(1)} %reshape.168), channel_id=2, replica_groups=mesh['ep'=16,'tp'=2] {'tp'}, dimensions={0}, use_global_device_ids=true | all-gather | bytes 4608 | tf_op jit(solution)/shard_map/all_gather | solution.py:88
  145.2 7.3 %all-to-all-start.5 = ((bf16[16,24,1]{1,2,0:T(2,128)(2,1)}), bf16[16,24,1]{1,2,0:T(2,128)(2,1)S(1)}, u32[]{:S(2)}, u32[]{:S(2)}) async-start(bf16[16,24,1]{1,2,0:T(2,128)(2,1)} %convert_element_type.96), calls=%async_computation.5 | async-start | bytes 16384 | tf_op jit(solution)/shard_map/all_to_all | solution.py:91
  152.6 3.3 %reduce_sum.55 = bf16[384,1024]{1,0:T(8,128)(2,1)} reduce(f32[384,2,1024]{2,0,1:T(8,128)} %all-to-all-done.3, f32[]{:T(128)} %constant.43.clone.1), dimensions={1}, to_apply=%region_3.5 | reduce | flops 393216 | bytes 3932164 | tf_op jit(solution)/shard_map/reduce_sum | solution.py:85
  155.8 1.4 all-to-all-done.5
  157.3 5.2 %all-to-all-start.4 = ((bf16[16,24,1024]{2,1,0:T(8,128)(2,1)}), bf16[16,24,1024]{2,1,0:T(8,128)(2,1)S(1)}, u32[]{:S(2)}, u32[]{:S(2)}) async-start(bf16[16,24,1024]{2,1,0:T(8,128)(2,1)} %bitcast.48), calls=%async_computation.4 | async-start | bytes 1572864 | tf_op jit(solution)/shard_map/all_to_all | solution.py:90
  164.0 3.0 %convolution_bitcast_fusion.1 = f32[1,2048,256]{2,1,0:T(8,128)} fusion(bf16[384,2048]{1,0:T(8,128)(2,1)S(1)} %copy-done.1, bf16[384,256]{0,1:T(8,128)(2,1)} %copy-done.10), kind=kOutput, calls=%fused_computation.9 | convolution fusion | flops 402653184 | bytes 3866624 | tf_op jit(solution)/shard_map/dot_general | solution.py:72
  167.1 2.1 %convolution_bitcast_fusion.2 = f32[1,2048,256]{2,1,0:T(8,128)} fusion(bf16[384,2048]{1,0:T(8,128)(2,1)S(1)} %copy-done.1, bf16[384,256]{0,1:T(8,128)(2,1)S(1)} %copy-done.9), kind=kOutput, calls=%fused_computation.10 | convolution fusion | flops 402653184 | bytes 3866624 | tf_op jit(solution)/shard_map/dot_general | solution.py:69
  169.2 2.1 %convolution_bitcast_fusion = f32[1,256,2048]{2,1,0:T(8,128)} fusion(bf16[384,2048]{1,0:T(8,128)(2,1)S(1)} %copy-done.3, f32[384]{0:T(512)S(1)} %reshape.116, f32[384,256]{0,1:T(8,128)S(1)} %copy-done.7, f32[384,256]{0,1:T(8,128)S(1)} %copy-done.5), kind=kOutput, calls=%fused_computation.8 | convolution fusion | flops 403341312 | bytes 4457984 | tf_op jit(solution)/shard_map/dot_general | solution.py:75
  171.4 1.9 %gather_fusion.1 = bf16[256]{0:T(256)(128)(2,1)S(1)} fusion(bf16[384]{0:T(512)(128)(2,1)S(1)} %all_to_all.57, s32[1024]{0:T(1024)S(1)} %pad_clamp_fusion), kind=kCustom, calls=%fused_computation.3 | custom fusion | bytes 2048 | tf_op jit(solution)/shard_map/jit(_take)/gather | solution.py:96
  174.9 7.3 %all-to-all-done.4 = bf16[16,24,1024]{2,1,0:T(8,128)(2,1)S(1)} async-done(((bf16[16,24,1024]{2,1,0:T(8,128)(2,1)}), bf16[16,24,1024]{2,1,0:T(8,128)(2,1)S(1)}, u32[]{:S(2)}, u32[]{:S(2)}) %all-to-all-start.4) | async-done | bytes 786464 | tf_op jit(solution)/shard_map/all_to_all | solution.py:90
  183.5 2.2 %convert_reduce_fusion = f32[128,1024]{1,0:T(8,128)} fusion(bf16[128,2,1024]{2,1,0:T(2,128)(2,1)S(1)} %gather.16, pred[128,2]{1,0:T(8,128)(4,1)S(1)} %get-tuple-element.20), kind=kLoop, calls=%fused_computation.22 | loop fusion | flops 655360 | bytes 1048832 | tf_op jit(solution)/shard_map/reduce_sum | solution.py:94
  (74 shorter events, 11.3 us)
Async XLA Ops:
  7.2 70.9 %copy-start = (bf16[1,2048,256]{2,1,0:T(8,128)(2,1)S(1)}, bf16[1,2048,256]{2,1,0:T(8,128)(2,1)}, u32[]{:S(2)}) copy-start(bf16[1,2048,256]{2,1,0:T(8,128)(2,1)} %param.17) | copy-start | bytes 3145732
  7.2 70.9 %all-gather.7.cloned.1.call-start = ((), (), s32[]{:S(2)}) async-start(), calls=%async_computation.7 | async-start | bytes 2359296 | tf_op jit(solution)/shard_map/all_gather | solution.py:45
  9.4 57.6 %copy-start.13 = (s32[256,1]{0,1:T(1,128)}, s32[256,1]{0,1:T(1,128)S(1)}, u32[]{:S(2)}) copy-start(s32[256,1]{0,1:T(1,128)S(1)} %compare_select_fusion.1) | copy-start | bytes 3076
  42.6 24.1 %copy-start.12 = (f32[128,2]{0,1:T(2,128)S(1)}, f32[128,2]{0,1:T(2,128)}, u32[]{:S(2)}) copy-start(f32[128,2]{0,1:T(2,128)} %param.14) | copy-start | bytes 3076
  42.6 24.1 %copy-start.14 = (f32[128]{0:T(128)S(1)}, f32[128]{0:T(128)}, u32[]{:S(2)}) copy-start(f32[128]{0:T(128)} %param.13) | copy-start | bytes 1540
  42.6 54.7 %all-gather.5.cloned.1.call-start = ((), (), s32[]{:S(2)}) async-start(), calls=%async_computation.6 | async-start | bytes 2359296 | tf_op jit(solution)/shard_map/all_gather | solution.py:46
  78.1 2.3 %copy-start.1 = (bf16[384,2048]{1,0:T(8,128)(2,1)S(1)}, bf16[384,2048]{1,0:T(8,128)(2,1)}, u32[]{:S(2)}) copy-start(bf16[384,2048]{1,0:T(8,128)(2,1)} %all-gather.7.cloned.1.call-done) | copy-start | bytes 4718596
  80.5 19.4 %copy-start.4 = (f32[384,256]{0,1:T(8,128)}, f32[384,256]{0,1:T(8,128)S(1)}, u32[]{:S(2)}) copy-start(f32[384,256]{0,1:T(8,128)S(1)} %fusion.3) | copy-start | bytes 1179652
  82.6 17.3 %copy-start.6 = (f32[384,256]{0,1:T(8,128)}, f32[384,256]{0,1:T(8,128)S(1)}, u32[]{:S(2)}) copy-start(f32[384,256]{0,1:T(8,128)S(1)} %fusion.6) | copy-start | bytes 1179652
  99.9 0.7 copy-start.8
  99.9 0.7 copy-start.10
  99.9 1.4 copy-start.2
  103.8 41.4 %all-to-all-start.3 = ((f32[384,2,1024]{2,0,1:T(8,128)}), f32[384,2,1024]{2,0,1:T(8,128)}, u32[]{:S(2)}, u32[]{:S(2)}) async-start(f32[384,2,1024]{2,0,1:T(8,128)} %bitcast.45), calls=%async_computation.3 | async-start | bytes 6291456 | tf_op jit(solution)/shard_map/all_to_all | solution.py:84
  145.2 12.0 %all-to-all-start.5 = ((bf16[16,24,1]{1,2,0:T(2,128)(2,1)}), bf16[16,24,1]{1,2,0:T(2,128)(2,1)S(1)}, u32[]{:S(2)}, u32[]{:S(2)}) async-start(bf16[16,24,1]{1,2,0:T(2,128)(2,1)} %convert_element_type.96), calls=%async_computation.5 | async-start | bytes 16384 | tf_op jit(solution)/shard_map/all_to_all | solution.py:91
  157.3 24.9 %all-to-all-start.4 = ((bf16[16,24,1024]{2,1,0:T(8,128)(2,1)}), bf16[16,24,1024]{2,1,0:T(8,128)(2,1)S(1)}, u32[]{:S(2)}, u32[]{:S(2)}) async-start(bf16[16,24,1024]{2,1,0:T(8,128)(2,1)} %bitcast.48), calls=%async_computation.4 | async-start | bytes 1572864 | tf_op jit(solution)/shard_map/all_to_all | solution.py:90
  164.0 3.0 %copy-start.9 = (bf16[384,256]{0,1:T(8,128)(2,1)S(1)}, bf16[384,256]{0,1:T(8,128)(2,1)}, u32[]{:S(2)}) copy-start(bf16[384,256]{0,1:T(8,128)(2,1)} %copy-done.8) | copy-start | bytes 589828
  167.1 2.1 %copy-start.3 = (bf16[384,2048]{1,0:T(8,128)(2,1)S(1)}, bf16[384,2048]{1,0:T(8,128)(2,1)}, u32[]{:S(2)}) copy-start(bf16[384,2048]{1,0:T(8,128)(2,1)} %all-gather.5.cloned.1.call-done) | copy-start | bytes 4718596
  167.1 2.1 %copy-start.5 = (f32[384,256]{0,1:T(8,128)S(1)}, f32[384,256]{0,1:T(8,128)}, u32[]{:S(2)}) copy-start(f32[384,256]{0,1:T(8,128)} %copy-done.4) | copy-start | bytes 1179652
  167.1 2.1 %copy-start.7 = (f32[384,256]{0,1:T(8,128)S(1)}, f32[384,256]{0,1:T(8,128)}, u32[]{:S(2)}) copy-start(f32[384,256]{0,1:T(8,128)} %copy-done.6) | copy-start | bytes 1179652
  169.2 4.3 %copy-start.11 = (s32[128,2]{1,0:T(8,128)S(1)}, s32[128,2]{1,0:T(8,128)}, u32[]{:S(2)}) copy-start(s32[128,2]{1,0:T(8,128)} %convert_element_type.81) | copy-start | bytes 3076
  169.2 4.3 %copy-start.15 = (f32[128]{0:T(128)S(1)}, f32[128]{0:T(128)}, u32[]{:S(2)}) copy-start(f32[128]{0:T(128)} %param.13) | copy-start | bytes 1540
Sparse Core Ops, SparseCore 0:
  42.7 25.8 all-gather.6
  70.2 27.1 all-gather.4
